TPU v7x, 32 devices: a whole 2x2x4 slice. The times are simulated.
32 devices in a mesh: sp: 8 (over z, x), tp: 4 (over y, core).
Axes of the slice: x: 2, y: 2, z: 4, core: 2. Of those that a mesh axis runs over, the one named last changes fastest.
Arguments:
- mixer_out: bfloat16 [1024, 2048], P('sp'), may hold values from -6 to 6
- out_grad: bfloat16 [1024, 2048], P('sp'), may hold values from -2 to 2
- route_ids: int32 [1024, 2], P('sp'), may hold values from 0 to 7, all different within a row; in each aligned block of 128 rows (0 to 127, 128 to 255, ...) at most 64 rows name the same one
- route_weights: float32 [1024, 2], P('sp'), may hold values from 0.2 to 1.2
- gate_branch: bfloat16 [1024, 2048], P('sp', 'tp'), may hold values from -4 to 4
- states: float32 [1024, 2048], P('sp', 'tp'), may hold values from -6 to 6
- decay: float32 [1024, 2048], P('sp', 'tp'), may hold values from 0 to 1
- w_proj: bfloat16 [2048, 2048], P(None, 'tp'), may hold values from -0.125 to 0.125
- w_gate: bfloat16 [8, 2048, 2048], P('sp', 'tp'), may hold values from -0.125 to 0.125
- w_up: bfloat16 [8, 2048, 2048], P('sp', 'tp'), may hold values from -0.125 to 0.125
- w_down: bfloat16 [8, 2048, 2048], P('sp', 'tp'), may hold values from -0.125 to 0.125
Outputs:
- grad_w_gate: bfloat16 [8, 2048, 2048], P('sp', 'tp')
- grad_w_up: bfloat16 [8, 2048, 2048], P('sp', 'tp')
- grad_w_down: bfloat16 [8, 2048, 2048], P('sp', 'tp')
- grad_w_proj: float32 [2048, 2048], P('sp', 'tp')
- grad_branch: bfloat16 [1024, 2048], P('sp', 'tp')
- grad_drive: float32 [1024, 2048], P('sp', 'tp')
- grad_decay: float32 [1024, 2048], P('sp', 'tp')
Inputs may be any that keep to these rules, and one draw needn't show every extreme that they name: `route_ids`: each row names 2 different experts. In the rows of one index of sp no expert is named more than 64 times, a bound that some block reaches.
All inputs are finite; a program needn't handle non-finite values.
Results may differ from a plain program's by a relative error of at most 0.02.
Values may be sent and summed in bfloat16 or wider, within the bound.
A program may use at most 64 MiB of HBM per device.

v0:
```python
import jax
import jax.numpy as jnp
from jax import lax
from jax.sharding import PartitionSpec as P


def entering(value, axis, join, neutral):
    count, mine = (lax.axis_size(axis), lax.axis_index(axis))
    pieces = jax.tree.map(lambda part: lax.all_gather(part, axis), value)
    pieces = jax.tree.map(lambda part: part[::-1], pieces)
    mine = count - 1 - mine
    so_far = jax.tree.map(
        lambda part, zero: jnp.full_like(part, 0) + jnp.asarray(zero, part.dtype), value, neutral
    )

    def lap(position, so_far):
        longer = join(so_far, jax.tree.map(lambda part: part[position], pieces))
        return jax.tree.map(lambda new, old: jnp.where(position < mine, new, old), longer, so_far)

    return lax.fori_loop(0, count - 1, lap, so_far)


def shifted(block, axis, distance):
    devices = range(lax.axis_size(axis))
    route = [(i - distance, i) for i in devices if i - distance in devices]
    return lax.ppermute(block, axis, route)


def linear_combine(earlier, later):
    return (earlier[0] * later[0], later[0] * earlier[1] + later[1])


def chain_combine(earlier, later):
    return (later[0] * earlier[0], later[1] + later[0] * earlier[1])


def expert_grads(inputs, cotangents, w_gate, w_up, w_down):
    gate_pre = jnp.einsum("esd,efd->esf", inputs, w_gate, preferred_element_type=jnp.float32)
    up_pre = jnp.einsum("esd,efd->esf", inputs, w_up, preferred_element_type=jnp.float32)
    sigmoid_gate = jax.nn.sigmoid(gate_pre)
    silu_gate = gate_pre * sigmoid_gate
    hidden = (silu_gate * up_pre).astype(jnp.bfloat16)
    hidden_grad = jnp.einsum("esd,efd->esf", cotangents, w_down, preferred_element_type=jnp.float32)
    up_grad = (hidden_grad * silu_gate).astype(jnp.bfloat16)
    gate_grad = (
        hidden_grad * up_pre * sigmoid_gate * (1.0 + gate_pre * (1.0 - sigmoid_gate))
    ).astype(jnp.bfloat16)
    grad_gate = jnp.einsum(
        "esf,esd->efd", gate_grad, inputs, preferred_element_type=jnp.float32
    ).astype(jnp.bfloat16)
    grad_up = jnp.einsum(
        "esf,esd->efd", up_grad, inputs, preferred_element_type=jnp.float32
    ).astype(jnp.bfloat16)
    grad_down = jnp.einsum(
        "esf,esd->efd", hidden, cotangents, preferred_element_type=jnp.float32
    ).astype(jnp.bfloat16)
    partial_value = jnp.einsum(
        "esf,efd->esd", gate_grad, w_gate, preferred_element_type=jnp.float32
    )
    partial_value = partial_value + jnp.einsum(
        "esf,efd->esd", up_grad, w_up, preferred_element_type=jnp.float32
    )
    return (grad_gate, grad_up, grad_down, partial_value.astype(jnp.bfloat16))


def local(
    mixer_out,
    out_grad,
    route_ids,
    route_weights,
    gate_branch,
    states,
    decay,
    w_proj,
    w_gate,
    w_up,
    w_down,
):
    tok_rows, model_width = mixer_out.shape
    top_count = route_ids.shape[1]
    local_experts = w_gate.shape[0]
    sp_size = lax.axis_size("sp")
    tp_size = lax.axis_size("tp")
    experts = local_experts * sp_size
    capacity = 2 * top_count * tok_rows // experts
    routes = tok_rows * top_count
    flat_ids = route_ids.reshape(-1)
    onehot = (flat_ids[:, None] == jnp.arange(experts, dtype=jnp.int32)[None, :]).astype(jnp.int32)
    position = jnp.sum(jnp.cumsum(onehot, axis=0) * onehot, axis=1) - 1
    bucket = flat_ids % local_experts * sp_size + flat_ids // local_experts
    slot_index = bucket * capacity + position
    source = (
        jnp.full((experts * capacity,), routes, jnp.int32)
        .at[slot_index]
        .set(jnp.arange(routes, dtype=jnp.int32))
    )
    scaled = (route_weights[:, :, None] * out_grad[:, None, :].astype(jnp.float32)).astype(
        jnp.bfloat16
    )
    scaled_pad = jnp.concatenate(
        [scaled.reshape(routes, model_width), jnp.zeros((1, model_width), jnp.bfloat16)], axis=0
    )
    token_pad = jnp.concatenate([mixer_out, jnp.zeros((1, model_width), jnp.bfloat16)], axis=0)
    slot_shape = (local_experts, sp_size, capacity, model_width)
    x_send = token_pad[source // top_count].reshape(slot_shape)
    c_send = scaled_pad[source].reshape(slot_shape)
    slot_share = capacity // tp_size
    first_slot = lax.axis_index("tp") * slot_share
    x_part = lax.dynamic_slice_in_dim(x_send, first_slot, slot_share, 2)
    c_part = lax.dynamic_slice_in_dim(c_send, first_slot, slot_share, 2)
    x_part, c_part = (
        lax.all_to_all(x_part, "sp", split_axis=1, concat_axis=1, tiled=True),
        lax.all_to_all(c_part, "sp", split_axis=1, concat_axis=1, tiled=True),
    )
    x_recv, c_recv = (
        lax.all_gather(x_part, "tp", axis=2, tiled=True),
        lax.all_gather(c_part, "tp", axis=2, tiled=True),
    )
    grad_gate, grad_up, grad_down, partial_value = expert_grads(
        x_recv.reshape(local_experts, -1, model_width),
        c_recv.reshape(local_experts, -1, model_width),
        w_gate,
        w_up,
        w_down,
    )
    pieces = lax.all_to_all(
        partial_value.reshape(slot_shape), "tp", split_axis=2, concat_axis=0, tiled=True
    )
    summed = jnp.sum(
        pieces.reshape(tp_size, local_experts, sp_size, slot_share, model_width).astype(
            jnp.float32
        ),
        axis=0,
    )
    returned = lax.all_to_all(
        summed.astype(jnp.bfloat16), "sp", split_axis=1, concat_axis=1, tiled=True
    ).astype(summed.dtype)
    offset = position - first_slot
    inside = ((offset >= 0) & (offset < slot_share)).astype(jnp.float32)
    index_part = bucket * slot_share + jnp.clip(offset, 0, slot_share - 1)
    picked = returned.reshape(-1, model_width)[index_part] * inside[:, None]
    token_part = jnp.sum(picked.reshape(tok_rows, top_count, model_width), axis=1)
    routed_total = lax.psum(token_part.astype(jnp.bfloat16), "tp").astype(jnp.float32)
    mid_grad = (out_grad.astype(jnp.float32) + routed_total).astype(jnp.bfloat16)
    gated = (gate_branch.astype(jnp.float32) * states).astype(jnp.bfloat16)
    proj_grad = lax.psum_scatter(
        lax.dot_general(
            mid_grad, gated, (((0,), (0,)), ((), ())), preferred_element_type=jnp.float32
        ).astype(jnp.bfloat16),
        "sp",
        scatter_dimension=0,
        tiled=True,
    ).astype(jnp.float32)
    act_grad = jnp.dot(mid_grad, w_proj, preferred_element_type=jnp.float32)
    branch_grad = (act_grad * states).astype(jnp.bfloat16)
    state_grad = act_grad * gate_branch.astype(jnp.float32)
    channels = decay.shape[1]
    next_decay = jnp.concatenate([decay[1:], jnp.ones((1, channels), jnp.float32)], axis=0)
    decay_prod, local_grad = lax.associative_scan(
        linear_combine, (next_decay[::-1], state_grad[::-1]), axis=0
    )
    decay_prod = decay_prod[::-1]
    local_grad = local_grad[::-1]
    head_decay = decay[0]
    carried = entering(
        (head_decay * decay_prod[0], head_decay * local_grad[0]),
        "sp",
        chain_combine,
        (jnp.ones_like(head_decay), jnp.zeros_like(head_decay)),
    )
    drive_grad = local_grad + decay_prod * carried[1][None, :]
    before = shifted(states[-1:], "sp", 1)
    previous = jnp.concatenate([before, states[:-1]], axis=0)
    decay_grad = drive_grad * previous
    return (grad_gate, grad_up, grad_down, proj_grad, branch_grad, drive_grad, decay_grad)


def solution(mesh):
    placed = (
        P("sp", None),
        P("sp", None),
        P("sp", None),
        P("sp", None),
        P("sp", "tp"),
        P("sp", "tp"),
        P("sp", "tp"),
        P(None, "tp"),
        P("sp", "tp", None),
        P("sp", "tp", None),
        P("sp", "tp", None),
    )
    return jax.shard_map(
        local,
        mesh=mesh,
        in_specs=placed,
        out_specs=(
            P("sp", "tp", None),
            P("sp", "tp", None),
            P("sp", "tp", None),
            P("sp", "tp"),
            P("sp", "tp"),
            P("sp", "tp"),
            P("sp", "tp"),
        ),
        check_vma=False,
    )
```

profile of v0, /device:TPU:0, one launch (start us, length us, event | category | flops | bytes accessed | tf_op | source)
XLA Modules:
  0.0 276.9 jit_solution(13569955936952840303)
XLA Ops:
  13.2 3.3 %gather_fusion.1 = bf16[512,2048]{1,0:T(8,128)(2,1)} fusion(bf16[129,2048]{1,0:T(8,128)(2,1)S(1)} %concatenate.49, s32[1024]{0:T(1024)S(1)} %get-tuple-element.176), kind=kCustom, calls=%fused_computation.1 | custom fusion | bytes 4196352 | tf_op jit(solution)/shard_map/gather | solution.py:105
  17.6 21.7 %all_to_all.27 = bf16[1,8,16,2048]{3,2,0,1:T(8,128)(2,1)} all-to-all(bf16[1,8,16,2048]{3,2,0,1:T(8,128)(2,1)S(1)} %constant_dynamic-slice_fusion.2), channel_id=1, replica_groups=mesh['sp'=8,'tp'=4] {'sp'}, dimensions={1} | all-to-all | bytes 1048576 | tf_op jit(solution)/shard_map/all_to_all | solution.py:112
  39.4 2.4 mul.210
  41.8 3.7 %mul.211 = f32[256,2048]{1,0:T(8,128)} reshape(f32[128,2,2048]{2,1,0:T(2,128)} %mul.210) | data formatting | bytes 4194304 | tf_op jit(solution)/shard_map/mul | solution.py:97
  45.7 2.1 multiply_convert_fusion
  47.9 3.3 %gather_fusion = bf16[512,2048]{1,0:T(8,128)(2,1)} fusion(bf16[257,2048]{1,0:T(8,128)(2,1)S(1)} %concatenate.48, s32[1024]{0:T(1024)S(1)} %get-tuple-element.177), kind=kCustom, calls=%fused_computation | custom fusion | bytes 4196352 | tf_op jit(solution)/shard_map/gather | solution.py:106
  52.2 17.3 %all_to_all.28 = bf16[1,8,16,2048]{3,2,0,1:T(8,128)(2,1)} all-to-all(bf16[1,8,16,2048]{3,2,0,1:T(8,128)(2,1)S(1)} %constant_dynamic-slice_fusion.3), channel_id=1, replica_groups=mesh['sp'=8,'tp'=4] {'sp'}, dimensions={1} | all-to-all | bytes 1048576 | tf_op jit(solution)/shard_map/all_to_all | solution.py:113
  69.7 3.0 %fusion.5 = f32[512,512]{1,0:T(8,128)S(1)} fusion(bf16[512,2048]{1,0:T(8,128)(2,1)} %bitcast.85, bf16[1,512,2048]{2,1,0:T(8,128)(2,1)S(1)} %copy-done), kind=kOutput, calls=%fused_computation.17 | convolution fusion | flops 1073741824 | bytes 5242880 | tf_op jit(solution)/shard_map/esd,efd->esf/dot_general | solution.py:38
  72.7 2.2 fusion.8
  75.0 16.4 %all-gather.5.cloned.1.call-done = bf16[1,8,64,2048]{3,2,0,1:T(8,128)(2,1)} async-done(((bf16[1,8,16,2048]{3,2,0,1:T(8,128)(2,1)}), bf16[1,8,64,2048]{3,2,0,1:T(8,128)(2,1)}) %all-gather.5.cloned.1.call-update) | async-done | bytes 2097168 | tf_op jit(solution)/shard_map/all_gather | solution.py:117
  91.4 4.0 %multiply_convert_fusion.2 = (bf16[512,512]{1,0:T(8,128)(2,1)S(1)}, bf16[512,512]{1,0:T(8,128)(2,1)S(1)}) fusion(f32[512,512]{1,0:T(8,128)S(1)} %fusion.5, f32[512,512]{1,0:T(8,128)} %fusion.8, bf16[512,2048]{1,0:T(8,128)(2,1)} %bitcast.89, bf16[1,512,2048]{2,1,0:T(8,128)(2,1)} %param.23), kind=kOutput, calls=%fused_computation.28 | convolution fusion | flops 1077149696 | bytes 7340032 | tf_op jit(solution)/shard_map/esd,efd->esf/dot_general | solution.py:43
  98.7 2.5 copy.37
  101.2 3.7 %all-to-all-start.2 = ((bf16[1,8,64,2048]{3,1,0,2:T(8,128)(2,1)}), bf16[1,8,64,2048]{3,1,0,2:T(8,128)(2,1)S(1)}, u32[]{:S(2)}, u32[]{:S(2)}) async-start(bf16[1,8,64,2048]{3,1,0,2:T(8,128)(2,1)} %copy.37), calls=%async_computation.2 | async-start | bytes 4194304 | tf_op jit(solution)/shard_map/all_to_all | solution.py:126
  105.5 3.4 %collective-permute-start = (f32[1,512]{1,0:T(1,128)}, f32[1,512]{1,0:T(1,128)S(1)}, u32[]{:S(2)}, u32[]{:S(2)}) collective-permute-start(f32[1,512]{1,0:T(1,128)} %slice.319), channel_id=1, source_target_pairs={{0,4},{4,8},{8,12},{12,16},{16,20},{20,24},{24,28},{1,5},{5,9},{9,... | collective-permute-start | bytes 6152 | tf_op jit(solution)/shard_map/ppermute | solution.py:26
  108.9 21.7 %all-to-all-done.2 = bf16[1,8,64,2048]{3,1,0,2:T(8,128)(2,1)S(1)} async-done(((bf16[1,8,64,2048]{3,1,0,2:T(8,128)(2,1)}), bf16[1,8,64,2048]{3,1,0,2:T(8,128)(2,1)S(1)}, u32[]{:S(2)}, u32[]{:S(2)}) %all-to-all-start.2) | async-done | bytes 2097184 | tf_op jit(solution)/shard_map/all_to_all | solution.py:126
  132.1 5.6 %all-to-all-start.3 = ((bf16[1,8,16,2048]{3,2,0,1:T(8,128)(2,1)}), bf16[1,8,16,2048]{3,2,0,1:T(8,128)(2,1)S(1)}, u32[]{:S(2)}, u32[]{:S(2)}) async-start(bf16[1,8,16,2048]{3,2,0,1:T(8,128)(2,1)} %copy.38), calls=%async_computation.3 | async-start | bytes 1048576 | tf_op jit(solution)/shard_map/all_to_all | solution.py:135
  141.9 4.3 %fusion = bf16[1,512,2048]{2,1,0:T(8,128)(2,1)} fusion(bf16[512,512]{1,0:T(8,128)(2,1)S(1)} %copy-done.14, bf16[512,2048]{1,0:T(8,128)(2,1)} %bitcast.86), kind=kOutput, calls=%fused_computation.12 | convolution fusion | flops 1074790400 | bytes 4718592 | tf_op jit(solution)/shard_map/esf,esd->efd/dot_general | solution.py:48
  146.3 2.7 fusion.2
  149.0 3.0 %all-to-all-done.3 = bf16[1,8,16,2048]{3,2,0,1:T(8,128)(2,1)S(1)} async-done(((bf16[1,8,16,2048]{3,2,0,1:T(8,128)(2,1)}), bf16[1,8,16,2048]{3,2,0,1:T(8,128)(2,1)S(1)}, u32[]{:S(2)}, u32[]{:S(2)}) %all-to-all-start.3) | async-done | bytes 524320 | tf_op jit(solution)/shard_map/all_to_all | solution.py:135
  152.1 1.5 gather_fusion.2
  153.6 2.2 gather.14
  155.8 5.6 %multiply_reduce_fusion = bf16[128,2048]{1,0:T(8,128)(2,1)} fusion(f32[128,2,2048]{2,1,0:T(2,128)} %gather.14, f32[128,2]{1,0:T(8,128)S(1)} %copy-done.16), kind=kLoop, calls=%fused_computation.24 | loop fusion | flops 786432 | bytes 2622464 | tf_op jit(solution)/shard_map/reduce_sum | solution.py:142
  161.6 4.2 %fusion.1 = bf16[1,512,2048]{2,1,0:T(8,128)(2,1)} fusion(bf16[512,512]{1,0:T(8,128)(2,1)S(1)} %copy-done.9, bf16[512,2048]{1,0:T(8,128)(2,1)} %bitcast.87), kind=kOutput, calls=%fused_computation.13 | convolution fusion | flops 1074790400 | bytes 4718592 | tf_op jit(solution)/shard_map/esf,esd->efd/dot_general | solution.py:51
  165.8 27.5 %all-reduce.34.cloned.1.call-done = bf16[128,2048]{1,0:T(8,128)(2,1)} async-done(((bf16[128,2048]{1,0:T(8,128)(2,1)}), bf16[128,2048]{1,0:T(8,128)(2,1)}) %all-reduce.34.cloned.1.call-update) | async-done | bytes 524304 | tf_op jit(solution)/shard_map/psum | solution.py:143
  193.3 2.9 %convert_multiply_fusion = (f32[128,512]{1,0:T(8,128)S(1)}, bf16[128,512]{1,0:T(8,128)(2,1)}) fusion(bf16[128,512]{1,0:T(8,128)(2,1)S(1)} %copy-done.10, f32[128,512]{1,0:T(8,128)S(1)} %copy-done.4, bf16[2048,512]{1,0:T(8,128)(2,1)} %param.20, bf16[128,2048]{1,0:T(8,128)(2,1)} %all-reduce.34.cloned.1.call-done, bf16[128,2048]{1,0:T(8,128)(2,1)S(1)} %copy-done.3), kind=kOutput, calls=%fused_computation.33 | convolution fusion | flops 269746176 | bytes 3932160 | tf_op jit(solution)/shard_map/dot_general | solution.py:154
  197.5 2.1 convolution_convert_fusion
  202.2 26.2 %all-gather = f32[8,1,512]{2,1,0:T(1,128)S(1)} all-gather(f32[1,1,512]{2,1,0:T(1,128)S(1)} %get-tuple-element.137), channel_id=1, replica_groups=mesh['sp'=8,'tp'=4] {'sp'}, dimensions={0}, use_global_device_ids=true | all-gather | bytes 18432 | tf_op jit(solution)/shard_map/all_gather | solution.py:9
  228.5 26.1 %all-gather.1 = f32[8,1,512]{2,1,0:T(1,128)S(1)} all-gather(f32[1,1,512]{2,1,0:T(1,128)S(1)} %get-tuple-element.136), channel_id=1, replica_groups=mesh['sp'=8,'tp'=4] {'sp'}, dimensions={0}, use_global_device_ids=true | all-gather | bytes 18432 | tf_op jit(solution)/shard_map/all_gather | solution.py:9
  256.6 1.7 rev.14
  258.3 1.7 rev.15
  260.9 7.6 %reduce-scatter.2.cloned.1.call-done = bf16[256,512]{1,0:T(8,128)(2,1)} async-done(((bf16[2048,512]{1,0:T(8,128)(2,1)}), bf16[256,512]{1,0:T(8,128)(2,1)}) %reduce-scatter.2.cloned.1.call-update) | async-done | bytes 262160 | tf_op jit(solution)/shard_map/reduce_scatter | solution.py:146
  268.5 1.8 convert_element_type.103
  (227 shorter events, 24.5 us)
Async XLA Ops:
  7.2 62.5 %copy-start = (bf16[1,512,2048]{2,1,0:T(8,128)(2,1)S(1)}, bf16[1,512,2048]{2,1,0:T(8,128)(2,1)}, u32[]{:S(2)}) copy-start(bf16[1,512,2048]{2,1,0:T(8,128)(2,1)} %param.21) | copy-start | bytes 6291460
  7.2 62.4 %all-gather.7.cloned.1.call-start = ((), (), s32[]{:S(2)}) async-start(), calls=%async_computation.6 | async-start | bytes 2621440 | tf_op jit(solution)/shard_map/all_gather | solution.py:116
  16.4 22.9 %copy-start.2 = (bf16[128,2048]{1,0:T(8,128)(2,1)S(1)}, bf16[128,2048]{1,0:T(8,128)(2,1)}, u32[]{:S(2)}) copy-start(bf16[128,2048]{1,0:T(8,128)(2,1)} %param.14) | copy-start | bytes 1572868
  39.3 52.1 %all-gather.5.cloned.1.call-start = ((), (), s32[]{:S(2)}) async-start(), calls=%async_computation.5 | async-start | bytes 2621440 | tf_op jit(solution)/shard_map/all_gather | solution.py:117
  41.7 3.7 %copy-start.17 = (f32[128,2]{0,1:T(2,128)S(1)}, f32[128,2]{0,1:T(2,128)}, u32[]{:S(2)}) copy-start(f32[128,2]{0,1:T(2,128)} %param.16) | copy-start | bytes 3076
  69.6 3.1 %copy-start.6 = (bf16[1,512,2048]{2,1,0:T(8,128)(2,1)S(1)}, bf16[1,512,2048]{2,1,0:T(8,128)(2,1)}, u32[]{:S(2)}) copy-start(bf16[1,512,2048]{2,1,0:T(8,128)(2,1)} %param.22) | copy-start | bytes 6291460
  69.6 3.0 %copy-start.18 = (bf16[1,8,64,2048]{3,2,0,1:T(8,128)(2,1)S(1)}, bf16[1,8,64,2048]{3,2,0,1:T(8,128)(2,1)}, u32[]{:S(2)}) copy-start(bf16[1,8,64,2048]{3,2,0,1:T(8,128)(2,1)} %all-gather.7.cloned.1.call-done) | copy-start | bytes 6291460
  72.7 18.7 %copy-start.20 = (f32[512,512]{1,0:T(8,128)}, f32[512,512]{1,0:T(8,128)S(1)}, u32[]{:S(2)}) copy-start(f32[512,512]{1,0:T(8,128)S(1)} %fusion.5) | copy-start | bytes 3145732
  95.4 1.3 copy-start.13
  95.5 1.3 copy-start.8
  95.5 2.0 copy-start.7
  101.2 3.8 %copy-start.4 = (f32[128,512]{1,0:T(8,128)S(1)}, f32[128,512]{1,0:T(8,128)}, u32[]{:S(2)}) copy-start(f32[128,512]{1,0:T(8,128)} %param.18) | copy-start | bytes 786436
  101.2 29.4 %all-to-all-start.2 = ((bf16[1,8,64,2048]{3,1,0,2:T(8,128)(2,1)}), bf16[1,8,64,2048]{3,1,0,2:T(8,128)(2,1)S(1)}, u32[]{:S(2)}, u32[]{:S(2)}) async-start(bf16[1,8,64,2048]{3,1,0,2:T(8,128)(2,1)} %copy.37), calls=%async_computation.2 | async-start | bytes 4194304 | tf_op jit(solution)/shard_map/all_to_all | solution.py:126
  105.5 154.5 %collective-permute-start = (f32[1,512]{1,0:T(1,128)}, f32[1,512]{1,0:T(1,128)S(1)}, u32[]{:S(2)}, u32[]{:S(2)}) collective-permute-start(f32[1,512]{1,0:T(1,128)} %slice.319), channel_id=1, source_target_pairs={{0,4},{4,8},{8,12},{12,16},{16,20},{20,24},{24,28},{1,5},{5,9},{9,... | collective-permute-start | bytes 6152 | tf_op jit(solution)/shard_map/ppermute | solution.py:26
  130.6 7.5 %copy-start.15 = (f32[128,512]{1,0:T(8,128)S(1)}, f32[128,512]{1,0:T(8,128)}, u32[]{:S(2)}) copy-start(f32[128,512]{1,0:T(8,128)} %param.19) | copy-start | bytes 786436
  132.1 9.8 %copy-start.14 = (bf16[512,512]{1,0:T(8,128)(2,1)S(1)}, bf16[512,512]{1,0:T(8,128)(2,1)}, u32[]{:S(2)}) copy-start(bf16[512,512]{1,0:T(8,128)(2,1)} %copy-done.13) | copy-start | bytes 1572868
  132.1 19.9 %all-to-all-start.3 = ((bf16[1,8,16,2048]{3,2,0,1:T(8,128)(2,1)}), bf16[1,8,16,2048]{3,2,0,1:T(8,128)(2,1)S(1)}, u32[]{:S(2)}, u32[]{:S(2)}) async-start(bf16[1,8,16,2048]{3,2,0,1:T(8,128)(2,1)} %copy.38), calls=%async_computation.3 | async-start | bytes 1048576 | tf_op jit(solution)/shard_map/all_to_all | solution.py:135
  137.7 55.6 %all-reduce.34.cloned.1.call-start = ((), (), s32[]{:S(2)}) async-start(), calls=%async_computation.7 | async-start | bytes 1048576 | tf_op jit(solution)/shard_map/psum | solution.py:143
  141.9 4.4 %copy-start.19 = (bf16[1,8,64,2048]{3,2,0,1:T(8,128)(2,1)S(1)}, bf16[1,8,64,2048]{3,2,0,1:T(8,128)(2,1)}, u32[]{:S(2)}) copy-start(bf16[1,8,64,2048]{3,2,0,1:T(8,128)(2,1)} %all-gather.5.cloned.1.call-done) | copy-start | bytes 6291460
  141.9 4.4 %copy-start.21 = (f32[512,512]{1,0:T(8,128)S(1)}, f32[512,512]{1,0:T(8,128)}, u32[]{:S(2)}) copy-start(f32[512,512]{1,0:T(8,128)} %copy-done.20) | copy-start | bytes 3145732
  141.9 4.4 %copy-start.22 = (f32[512,512]{1,0:T(8,128)S(1)}, f32[512,512]{1,0:T(8,128)}, u32[]{:S(2)}) copy-start(f32[512,512]{1,0:T(8,128)} %fusion.8) | copy-start | bytes 3145732
  153.6 2.3 copy-start.16
  155.8 5.7 %copy-start.9 = (bf16[512,512]{1,0:T(8,128)(2,1)S(1)}, bf16[512,512]{1,0:T(8,128)(2,1)}, u32[]{:S(2)}) copy-start(bf16[512,512]{1,0:T(8,128)(2,1)} %copy-done.8) | copy-start | bytes 1572868
  161.5 31.8 %copy-start.3 = (bf16[128,2048]{1,0:T(8,128)(2,1)S(1)}, bf16[128,2048]{1,0:T(8,128)(2,1)}, u32[]{:S(2)}) copy-start(bf16[128,2048]{1,0:T(8,128)(2,1)} %param.14) | copy-start | bytes 1572868
  161.5 31.8 %copy-start.10 = (bf16[128,512]{1,0:T(8,128)(2,1)S(1)}, bf16[128,512]{1,0:T(8,128)(2,1)}, u32[]{:S(2)}) copy-start(bf16[128,512]{1,0:T(8,128)(2,1)} %param.17) | copy-start | bytes 393220
  161.5 107.0 %reduce-scatter.2.cloned.1.call-start = ((), (), s32[]{:S(2)}) async-start(), calls=%async_computation.8 | async-start | bytes 2359296 | tf_op jit(solution)/shard_map/reduce_scatter | solution.py:146
  165.8 30.9 %copy-start.11 = (f32[64,512]{1,0:T(8,128)S(1)}, f32[64,512]{1,0:T(8,128)}, u32[]{:S(2)}) copy-start(f32[64,512]{1,0:T(8,128)} %slice.251) | copy-start | bytes 393220
  196.2 1.3 copy-start.5
  200.2 0.9 copy-start.12
  255.1 15.2 %copy-start.1 = (bf16[1,512,2048]{2,1,0:T(8,128)(2,1)S(1)}, bf16[1,512,2048]{2,1,0:T(8,128)(2,1)}, u32[]{:S(2)}) copy-start(bf16[1,512,2048]{2,1,0:T(8,128)(2,1)} %param.21) | copy-start | bytes 6291460
Sparse Core Ops, SparseCore 0:
  39.4 21.5 all-gather.6
  69.7 21.6 all-gather.4
  161.6 31.6 all-reduce.33
  199.7 68.7 reduce-scatter.1
where the time goes:
time: 278 us; the launch traced here: 277 us
  blocking collectives  91.4 us (33%)
  waiting for transfers between devices  76.3 us (27%)
  local copies, waits for them, and re-layouts  37.5 us (13%)
  matrix products  28.1 us (10%)
  other arithmetic  15.3 us (6%)
  between operations  14.8 us (5%)
  starting transfers between devices  13.1 us (5%)
    all_gather x2, blocking collectives, entering(): pieces = jax.tree.map(lambda part: lax.all_gather(part, axis), value)  52.4 us
    psum x1, waiting for transfers between devices, local(): lax.psum(token_part.astype(jnp.bfloat16), 'tp').astype(jnp.float32)  27.5 us
    all_to_all x1, blocking collectives, local(): lax.all_to_all(x_part, 'sp', split_axis=1, concat_axis=1, tiled=True)  21.7 us
    all_to_all x1, waiting for transfers between devices, local(): lax.all_to_all(partial_value.reshape(slot_shape), 'tp', split_axis=2, con...  21.7 us
    all_to_all x1, blocking collectives, local(): lax.all_to_all(c_part, 'sp', split_axis=1, concat_axis=1, tiled=True)  17.3 us
    all_gather x1, waiting for transfers between devices, local(): lax.all_gather(c_part, 'tp', axis=2, tiled=True)  16.4 us
    reduce_scatter x1, waiting for transfers between devices, local(): lax.psum_scatter(lax.dot_general(mid_grad, gated, (((0,), (0,)), ((), ())...  7.59 us
    mul x3, local copies, waits for them, and re-layouts, local(): route_weights[:, :, None] * out_grad[:, None, :].astype(jnp.float32)  6.17 us
  transfers between devices with their start and end apart: 7, of which 5 were waited for; matrix products, arithmetic and copies ran while one was open for 21% of the time, Pallas kernels for 0%

commit v1 on v0

--- a/solution.py
+++ b/solution.py
@@ -140,7 +140,9 @@
     index_part = bucket * slot_share + jnp.clip(offset, 0, slot_share - 1)
     picked = returned.reshape(-1, model_width)[index_part] * inside[:, None]
     token_part = jnp.sum(picked.reshape(tok_rows, top_count, model_width), axis=1)
-    routed_total = lax.psum(token_part.astype(jnp.bfloat16), "tp").astype(jnp.float32)
+    routed_total = jnp.sum(lax.all_gather(token_part.astype(jnp.bfloat16), "tp"), axis=0).astype(
+        jnp.float32
+    )
     mid_grad = (out_grad.astype(jnp.float32) + routed_total).astype(jnp.bfloat16)
     gated = (gate_branch.astype(jnp.float32) * states).astype(jnp.bfloat16)
     proj_grad = lax.psum_scatter(

time: 278 us -> 266 us (0.957)
  waiting for transfers between devices: 76.3 us -> 44.1 us
  blocking collectives: 91.4 us -> 120 us
  local copies, waits for them, and re-layouts: 37.5 us -> 32.4 us
  starting transfers between devices: 13.1 us -> 9.61 us
    all_to_all x0 -> x1, blocking collectives: none -> 28.1 us  [local(): lax.all_to_all(partial_value.reshape(slot_shape), 'tp', split_axis=2, con...]
    psum x1 -> x0, waiting for transfers between devices: 27.5 us -> none  [local(): lax.psum(token_part.astype(jnp.bfloat16), 'tp').astype(jnp.float32)]
    all_to_all x1 -> x0, waiting for transfers between devices: 21.7 us -> none  [local(): lax.all_to_all(partial_value.reshape(slot_shape), 'tp', split_axis=2, con...]
    all_to_all x1, waiting for transfers between devices: 3.01 us -> 13.7 us  [local(): lax.all_to_all(summed.astype(jnp.bfloat16), 'sp', split_axis=1, concat_ax...]
    all_gather x0 -> x1, waiting for transfers between devices: none -> 6.58 us  [local(): lax.all_gather(token_part.astype(jnp.bfloat16), 'tp')]
    all_to_all x1 -> x0, starting transfers between devices: 3.74 us -> none  [local(): lax.all_to_all(partial_value.reshape(slot_shape), 'tp', split_axis=2, con...]
  transfers between devices with their start and end apart: 7 -> 6, of which waited for: 5 -> 4; matrix products, arithmetic and copies ran while one was open for 21% -> 17% of each run, Pallas kernels for 0% -> 0%
where the time goes in v1:
time: 266 us; the launch traced here: 265 us
  blocking collectives  120 us (45%)
  waiting for transfers between devices  44.1 us (17%)
  local copies, waits for them, and re-layouts  32.4 us (12%)
  matrix products  26.4 us (10%)
  other arithmetic  17.4 us (7%)
  between operations  14.8 us (6%)
  starting transfers between devices  9.61 us (4%)
    all_gather x2, blocking collectives, entering(): pieces = jax.tree.map(lambda part: lax.all_gather(part, axis), value)  52.5 us
    all_to_all x1, blocking collectives, local(): lax.all_to_all(partial_value.reshape(slot_shape), 'tp', split_axis=2, con...  28.1 us
    all_to_all x1, blocking collectives, local(): lax.all_to_all(x_part, 'sp', split_axis=1, concat_axis=1, tiled=True)  21.7 us
    all_to_all x1, blocking collectives, local(): lax.all_to_all(c_part, 'sp', split_axis=1, concat_axis=1, tiled=True)  17.3 us
    all_gather x1, waiting for transfers between devices, local(): lax.all_gather(c_part, 'tp', axis=2, tiled=True)  16.4 us
    all_to_all x1, waiting for transfers between devices, local(): lax.all_to_all(summed.astype(jnp.bfloat16), 'sp', split_axis=1, concat_ax...  13.7 us
    reduce_scatter x1, waiting for transfers between devices, local(): lax.psum_scatter(lax.dot_general(mid_grad, gated, (((0,), (0,)), ((), ())...  7.28 us
    all_gather x1, waiting for transfers between devices, local(): lax.all_gather(token_part.astype(jnp.bfloat16), 'tp')  6.58 us
  transfers between devices with their start and end apart: 6, of which 4 were waited for; matrix products, arithmetic and copies ran while one was open for 17% of the time, Pallas kernels for 0%

profile of v1, /device:TPU:0, one launch (start us, length us, event | category | flops | bytes accessed | tf_op | source)
XLA Modules:
  0.0 264.8 jit_solution(6914159957963554092)
XLA Ops:
  10.6 1.4 scatter_custom_fusion
  13.2 3.3 %gather_fusion.1 = bf16[512,2048]{1,0:T(8,128)(2,1)} fusion(bf16[129,2048]{1,0:T(8,128)(2,1)S(1)} %concatenate.49, s32[1024]{0:T(1024)S(1)} %get-tuple-element.176), kind=kCustom, calls=%fused_computation.1 | custom fusion | bytes 4196352 | tf_op jit(solution)/shard_map/gather | solution.py:105
  17.6 21.7 %all_to_all.27 = bf16[1,8,16,2048]{3,2,0,1:T(8,128)(2,1)} all-to-all(bf16[1,8,16,2048]{3,2,0,1:T(8,128)(2,1)S(1)} %constant_dynamic-slice_fusion.2), channel_id=1, replica_groups=mesh['sp'=8,'tp'=4] {'sp'}, dimensions={1} | all-to-all | bytes 1048576 | tf_op jit(solution)/shard_map/all_to_all | solution.py:112
  39.4 2.4 mul.210
  41.8 3.7 %mul.211 = f32[256,2048]{1,0:T(8,128)} reshape(f32[128,2,2048]{2,1,0:T(2,128)} %mul.210) | data formatting | bytes 4194304 | tf_op jit(solution)/shard_map/mul | solution.py:97
  45.7 2.1 multiply_convert_fusion
  47.9 3.3 %gather_fusion = bf16[512,2048]{1,0:T(8,128)(2,1)} fusion(bf16[257,2048]{1,0:T(8,128)(2,1)S(1)} %concatenate.48, s32[1024]{0:T(1024)S(1)} %get-tuple-element.177), kind=kCustom, calls=%fused_computation | custom fusion | bytes 4196352 | tf_op jit(solution)/shard_map/gather | solution.py:106
  52.2 17.3 %all_to_all.28 = bf16[1,8,16,2048]{3,2,0,1:T(8,128)(2,1)} all-to-all(bf16[1,8,16,2048]{3,2,0,1:T(8,128)(2,1)S(1)} %constant_dynamic-slice_fusion.3), channel_id=1, replica_groups=mesh['sp'=8,'tp'=4] {'sp'}, dimensions={1} | all-to-all | bytes 1048576 | tf_op jit(solution)/shard_map/all_to_all | solution.py:113
  69.7 3.0 %fusion.5 = f32[512,512]{1,0:T(8,128)S(1)} fusion(bf16[512,2048]{1,0:T(8,128)(2,1)} %bitcast.87, bf16[1,512,2048]{2,1,0:T(8,128)(2,1)S(1)} %copy-done), kind=kOutput, calls=%fused_computation.17 | convolution fusion | flops 1073741824 | bytes 5242880 | tf_op jit(solution)/shard_map/esd,efd->esf/dot_general | solution.py:38
  72.7 2.2 fusion.8
  75.0 16.4 %all-gather.7.cloned.1.call-done = bf16[1,8,64,2048]{3,2,0,1:T(8,128)(2,1)} async-done(((bf16[1,8,16,2048]{3,2,0,1:T(8,128)(2,1)}), bf16[1,8,64,2048]{3,2,0,1:T(8,128)(2,1)}) %all-gather.7.cloned.1.call-update) | async-done | bytes 2097168 | tf_op jit(solution)/shard_map/all_gather | solution.py:117
  91.4 4.0 %multiply_convert_fusion.2 = (bf16[512,512]{1,0:T(8,128)(2,1)S(1)}, bf16[512,512]{1,0:T(8,128)(2,1)S(1)}) fusion(f32[512,512]{1,0:T(8,128)S(1)} %fusion.5, f32[512,512]{1,0:T(8,128)} %fusion.8, bf16[512,2048]{1,0:T(8,128)(2,1)} %bitcast.91, bf16[1,512,2048]{2,1,0:T(8,128)(2,1)} %param.23), kind=kOutput, calls=%fused_computation.28 | convolution fusion | flops 1077149696 | bytes 7340032 | tf_op jit(solution)/shard_map/esd,efd->esf/dot_general | solution.py:43
  99.9 28.1 %all_to_all.29 = bf16[1,8,64,2048]{3,1,0,2:T(8,128)(2,1)S(1)} all-to-all(bf16[1,8,64,2048]{3,1,0,2:T(8,128)(2,1)S(1)} %copy.46), channel_id=1, replica_groups=mesh['sp'=8,'tp'=4] {'tp'}, dimensions={2} | all-to-all | bytes 4194304 | tf_op jit(solution)/shard_map/all_to_all | solution.py:126
  129.5 5.5 %all-to-all-start.3 = ((bf16[1,8,16,2048]{3,2,0,1:T(8,128)(2,1)}), bf16[1,8,16,2048]{3,2,0,1:T(8,128)(2,1)S(1)}, u32[]{:S(2)}, u32[]{:S(2)}) async-start(bf16[1,8,16,2048]{3,2,0,1:T(8,128)(2,1)} %copy.47), calls=%async_computation.3 | async-start | bytes 1048576 | tf_op jit(solution)/shard_map/all_to_all | solution.py:135
  135.5 13.7 %all-to-all-done.3 = bf16[1,8,16,2048]{3,2,0,1:T(8,128)(2,1)S(1)} async-done(((bf16[1,8,16,2048]{3,2,0,1:T(8,128)(2,1)}), bf16[1,8,16,2048]{3,2,0,1:T(8,128)(2,1)S(1)}, u32[]{:S(2)}, u32[]{:S(2)}) %all-to-all-start.3) | async-done | bytes 524320 | tf_op jit(solution)/shard_map/all_to_all | solution.py:135
  149.3 1.5 gather_fusion.2
  150.8 2.2 gather.14
  153.0 5.7 %multiply_reduce_fusion = bf16[128,2048]{1,0:T(8,128)(2,1)} fusion(f32[128,2,2048]{2,1,0:T(2,128)} %gather.14, f32[128,2]{1,0:T(8,128)S(1)} %reshape.239), kind=kLoop, calls=%fused_computation.24 | loop fusion | flops 786432 | bytes 2622464 | tf_op jit(solution)/shard_map/reduce_sum | solution.py:142
  158.8 3.7 %collective-permute-start = (f32[1,512]{1,0:T(1,128)S(1)}, f32[1,512]{1,0:T(1,128)S(1)}, u32[]{:S(2)}, u32[]{:S(2)}) collective-permute-start(f32[1,512]{1,0:T(1,128)S(1)} %slice.319), channel_id=1, source_target_pairs={{0,4},{4,8},{8,12},{12,16},{16,20},{20,24},{24,28},{1,5},{5,9},{9,... | collective-permute-start | bytes 6152 | tf_op jit(solution)/shard_map/ppermute | solution.py:26
  163.4 4.5 %fusion = bf16[1,512,2048]{2,1,0:T(8,128)(2,1)} fusion(bf16[512,512]{1,0:T(8,128)(2,1)S(1)} %copy-done.11, bf16[512,2048]{1,0:T(8,128)(2,1)} %bitcast.88), kind=kOutput, calls=%fused_computation.12 | convolution fusion | flops 1074790400 | bytes 4718592 | tf_op jit(solution)/shard_map/esf,esd->efd/dot_general | solution.py:48
  167.9 2.6 fusion.1
  170.5 2.7 %fusion.2 = bf16[1,512,2048]{2,1,0:T(8,128)(2,1)} fusion(bf16[512,2048]{1,0:T(8,128)(2,1)S(1)} %bitcast.92, f32[512,512]{1,0:T(8,128)S(1)} %copy-done.19, f32[512,512]{1,0:T(8,128)S(1)} %copy-done.18), kind=kOutput, calls=%fused_computation.14 | convolution fusion | flops 1076363264 | bytes 6291456 | tf_op jit(solution)/shard_map/esf,esd->efd/dot_general | solution.py:54
  173.2 6.6 %all-gather.11.cloned.1.call-done = bf16[512,2048]{1,0:T(8,128)(2,1)} async-done(((bf16[128,2048]{1,0:T(8,128)(2,1)}), bf16[512,2048]{1,0:T(8,128)(2,1)}) %all-gather.11.cloned.1.call-update) | async-done | bytes 2097168 | tf_op jit(solution)/shard_map/all_gather | solution.py:143
  179.8 2.0 reduce_sum.48
  181.9 2.1 convolution_convert_fusion
  184.0 2.7 %convert_multiply_fusion = (f32[128,512]{1,0:T(8,128)S(1)}, bf16[128,512]{1,0:T(8,128)(2,1)}) fusion(bf16[128,512]{1,0:T(8,128)(2,1)S(1)} %copy-done.9, f32[128,512]{1,0:T(8,128)S(1)} %copy-done.4, bf16[2048,512]{1,0:T(8,128)(2,1)} %param.20, bf16[128,2048]{1,0:T(8,128)(2,1)S(1)} %reduce_sum.48, bf16[128,2048]{1,0:T(8,128)(2,1)S(1)} %copy-done.3), kind=kOutput, calls=%fused_computation.33 | convolution fusion | flops 269746176 | bytes 3932160 | tf_op jit(solution)/shard_map/dot_general | solution.py:156
  190.3 26.4 %all-gather.1 = f32[8,1,512]{2,1,0:T(1,128)S(1)} all-gather(f32[1,1,512]{2,1,0:T(1,128)S(1)} %get-tuple-element.137), channel_id=1, replica_groups=mesh['sp'=8,'tp'=4] {'sp'}, dimensions={0}, use_global_device_ids=true | all-gather | bytes 18432 | tf_op jit(solution)/shard_map/all_gather | solution.py:9
  216.7 26.1 %all-gather.2 = f32[8,1,512]{2,1,0:T(1,128)S(1)} all-gather(f32[1,1,512]{2,1,0:T(1,128)S(1)} %get-tuple-element.136), channel_id=1, replica_groups=mesh['sp'=8,'tp'=4] {'sp'}, dimensions={0}, use_global_device_ids=true | all-gather | bytes 18432 | tf_op jit(solution)/shard_map/all_gather | solution.py:9
  244.8 1.7 rev.14
  246.6 1.7 rev.15
  249.2 7.3 %reduce-scatter.2.cloned.1.call-done = bf16[256,512]{1,0:T(8,128)(2,1)} async-done(((bf16[2048,512]{1,0:T(8,128)(2,1)}), bf16[256,512]{1,0:T(8,128)(2,1)}) %reduce-scatter.2.cloned.1.call-update) | async-done | bytes 262160 | tf_op jit(solution)/shard_map/reduce_scatter | solution.py:148
  256.5 1.8 convert_element_type.116
  (221 shorter events, 20.5 us)
Async XLA Ops:
  7.2 62.5 %copy-start = (bf16[1,512,2048]{2,1,0:T(8,128)(2,1)S(1)}, bf16[1,512,2048]{2,1,0:T(8,128)(2,1)}, u32[]{:S(2)}) copy-start(bf16[1,512,2048]{2,1,0:T(8,128)(2,1)} %param.21) | copy-start | bytes 6291460
  7.2 62.4 %all-gather.9.cloned.1.call-start = ((), (), s32[]{:S(2)}) async-start(), calls=%async_computation.6 | async-start | bytes 2621440 | tf_op jit(solution)/shard_map/all_gather | solution.py:116
  16.4 22.9 %copy-start.2 = (bf16[128,2048]{1,0:T(8,128)(2,1)S(1)}, bf16[128,2048]{1,0:T(8,128)(2,1)}, u32[]{:S(2)}) copy-start(bf16[128,2048]{1,0:T(8,128)(2,1)} %param.14) | copy-start | bytes 1572868
  39.3 52.1 %all-gather.7.cloned.1.call-start = ((), (), s32[]{:S(2)}) async-start(), calls=%async_computation.5 | async-start | bytes 2621440 | tf_op jit(solution)/shard_map/all_gather | solution.py:117
  41.7 3.7 %copy-start.13 = (f32[128,2]{0,1:T(2,128)S(1)}, f32[128,2]{0,1:T(2,128)}, u32[]{:S(2)}) copy-start(f32[128,2]{0,1:T(2,128)} %param.16) | copy-start | bytes 3076
  69.6 3.1 %copy-start.5 = (bf16[1,512,2048]{2,1,0:T(8,128)(2,1)S(1)}, bf16[1,512,2048]{2,1,0:T(8,128)(2,1)}, u32[]{:S(2)}) copy-start(bf16[1,512,2048]{2,1,0:T(8,128)(2,1)} %param.22) | copy-start | bytes 6291460
  69.6 3.0 %copy-start.14 = (bf16[1,8,64,2048]{3,2,0,1:T(8,128)(2,1)S(1)}, bf16[1,8,64,2048]{3,2,0,1:T(8,128)(2,1)}, u32[]{:S(2)}) copy-start(bf16[1,8,64,2048]{3,2,0,1:T(8,128)(2,1)} %all-gather.9.cloned.1.call-done) | copy-start | bytes 6291460
  72.7 18.7 %copy-start.17 = (f32[512,512]{1,0:T(8,128)}, f32[512,512]{1,0:T(8,128)S(1)}, u32[]{:S(2)}) copy-start(f32[512,512]{1,0:T(8,128)S(1)} %fusion.5) | copy-start | bytes 3145732
  95.5 1.3 copy-start.10
  95.5 1.3 copy-start.7
  95.5 2.0 copy-start.6
  129.5 19.7 %all-to-all-start.3 = ((bf16[1,8,16,2048]{3,2,0,1:T(8,128)(2,1)}), bf16[1,8,16,2048]{3,2,0,1:T(8,128)(2,1)S(1)}, u32[]{:S(2)}, u32[]{:S(2)}) async-start(bf16[1,8,16,2048]{3,2,0,1:T(8,128)(2,1)} %copy.47), calls=%async_computation.3 | async-start | bytes 1048576 | tf_op jit(solution)/shard_map/all_to_all | solution.py:135
  135.0 44.8 %all-gather.11.cloned.1.call-start = ((), (), s32[]{:S(2)}) async-start(), calls=%async_computation.8 | async-start | bytes 2621440 | tf_op jit(solution)/shard_map/all_gather | solution.py:143
  153.0 5.8 %copy-start.4 = (f32[128,512]{1,0:T(8,128)S(1)}, f32[128,512]{1,0:T(8,128)}, u32[]{:S(2)}) copy-start(f32[128,512]{1,0:T(8,128)} %param.18) | copy-start | bytes 786436
  153.0 9.5 %copy-start.12 = (f32[128,512]{1,0:T(8,128)S(1)}, f32[128,512]{1,0:T(8,128)}, u32[]{:S(2)}) copy-start(f32[128,512]{1,0:T(8,128)} %param.19) | copy-start | bytes 786436
  158.7 4.7 %copy-start.11 = (bf16[512,512]{1,0:T(8,128)(2,1)S(1)}, bf16[512,512]{1,0:T(8,128)(2,1)}, u32[]{:S(2)}) copy-start(bf16[512,512]{1,0:T(8,128)(2,1)} %copy-done.10) | copy-start | bytes 1572868
  158.8 97.7 %reduce-scatter.2.cloned.1.call-start = ((), (), s32[]{:S(2)}) async-start(), calls=%async_computation.7 | async-start | bytes 2359296 | tf_op jit(solution)/shard_map/reduce_scatter | solution.py:148
  158.8 89.5 %collective-permute-start = (f32[1,512]{1,0:T(1,128)S(1)}, f32[1,512]{1,0:T(1,128)S(1)}, u32[]{:S(2)}, u32[]{:S(2)}) collective-permute-start(f32[1,512]{1,0:T(1,128)S(1)} %slice.319), channel_id=1, source_target_pairs={{0,4},{4,8},{8,12},{12,16},{16,20},{20,24},{24,28},{1,5},{5,9},{9,... | collective-permute-start | bytes 6152 | tf_op jit(solution)/shard_map/ppermute | solution.py:26
  163.4 4.5 %copy-start.8 = (bf16[512,512]{1,0:T(8,128)(2,1)S(1)}, bf16[512,512]{1,0:T(8,128)(2,1)}, u32[]{:S(2)}) copy-start(bf16[512,512]{1,0:T(8,128)(2,1)} %copy-done.7) | copy-start | bytes 1572868
  163.4 4.5 %copy-start.15 = (bf16[1,8,64,2048]{3,2,0,1:T(8,128)(2,1)S(1)}, bf16[1,8,64,2048]{3,2,0,1:T(8,128)(2,1)}, u32[]{:S(2)}) copy-start(bf16[1,8,64,2048]{3,2,0,1:T(8,128)(2,1)} %all-gather.9.cloned.1.call-done) | copy-start | bytes 6291460
  167.9 2.6 copy-start.16
  167.9 2.6 copy-start.18
  167.9 2.6 copy-start.19
  173.2 8.6 %copy-start.3 = (bf16[128,2048]{1,0:T(8,128)(2,1)S(1)}, bf16[128,2048]{1,0:T(8,128)(2,1)}, u32[]{:S(2)}) copy-start(bf16[128,2048]{1,0:T(8,128)(2,1)} %param.14) | copy-start | bytes 1572868
  173.2 8.6 %copy-start.9 = (bf16[128,512]{1,0:T(8,128)(2,1)S(1)}, bf16[128,512]{1,0:T(8,128)(2,1)}, u32[]{:S(2)}) copy-start(bf16[128,512]{1,0:T(8,128)(2,1)} %param.17) | copy-start | bytes 393220
  243.4 14.9 %copy-start.1 = (bf16[1,512,2048]{2,1,0:T(8,128)(2,1)S(1)}, bf16[1,512,2048]{2,1,0:T(8,128)(2,1)}, u32[]{:S(2)}) copy-start(bf16[1,512,2048]{2,1,0:T(8,128)(2,1)} %param.21) | copy-start | bytes 6291460
Sparse Core Ops, SparseCore 0:
  39.4 21.5 all-gather.8
  69.7 21.6 all-gather.6
  158.9 20.8 all-gather.10
  188.1 68.3 reduce-scatter.1
